TPU v7x, 32 devices: a whole 2x2x4 slice. The times are simulated.
32 devices in a mesh: grp: 2 (over x), sp: 4 (over z), tp: 4 (over y, core).
Axes of the slice: x: 2, y: 2, z: 4, core: 2. Of those that a mesh axis runs over, the one named last changes fastest.
Arguments:
- stream: bfloat16 [4096, 2560], P(None, ('grp', 'sp')), parts along dimension 1, may hold values from -6 to 6
- norm_gain: float32 [2, 4096], replicated, may hold values from 0.1 to 1.9
- value_weight: bfloat16 [2, 2048, 4096], P(None, 'tp'), may hold values from -0.09375 to 0.09375
- gate_weight: bfloat16 [2, 2048, 4096], P(None, 'tp'), may hold values from -0.09375 to 0.09375
- conv_kernel: float32 [2, 2048, 31], P(None, 'tp')
- conv_bias: float32 [2, 2048], P(None, 'tp'), may hold values from -3 to 3
- channel_gain: float32 [2, 2048], P(None, 'tp'), may hold values from 0.1 to 1.9
- channel_bias: float32 [2, 2048], P(None, 'tp'), may hold values from -3 to 3
- out_weight: bfloat16 [2, 4096, 2048], P(None, 'tp'), may hold values from -0.25 to 0.25
Outputs:
- result: bfloat16 [4096, 2560], P('tp', ('grp', 'sp')), parts along dimension 1
There are 2 independent parts, one for each index of `grp`. A program takes and returns all parts, laid end to end along the dimension named above; an argument that names none is the same for every part. Nothing has to cross between parts.
All inputs are finite; a program needn't handle non-finite values.
Results may differ from a plain program's by a relative error of at most 0.012.
Values may be sent and summed in bfloat16 or wider, within the bound.
A program may use at most 128 MiB of HBM per device.

v0:
```python
import jax
import jax.numpy as jnp
from jax import lax
from jax.sharding import PartitionSpec as P

K = 31
LAYERS = 2


epsilon = 1e-06


def shifted(value, axis, steps):
    count = lax.axis_size(axis)
    initial, last = (max(0, -steps), min(count, count - steps))
    return lax.ppermute(value, axis, [(source, source + steps) for source in range(initial, last)])


def depthwise(signal, kernel):
    out = lax.conv_general_dilated(
        signal[None],
        kernel[:, None, :],
        (1,),
        [(0, 0)],
        dimension_numbers=("NCW", "OIW", "NCW"),
        feature_group_count=kernel.shape[0],
        precision=lax.Precision.HIGHEST,
    )
    return out[0]


def norm_project(whole, gain, weights):
    scaling = lax.rsqrt(jnp.mean(whole * whole, axis=0, keepdims=True) + epsilon)
    normed = (whole * scaling * gain[:, None]).astype(jnp.bfloat16)
    return jnp.dot(weights, normed, preferred_element_type=jnp.float32)


def local(
    stream,
    norm_gain,
    value_weight,
    gate_weight,
    conv_kernel,
    conv_bias,
    channel_gain,
    channel_bias,
    out_weight,
):
    shard_channels = value_weight.shape[1]
    total_channels = shard_channels * lax.axis_size("tp")
    shard_features = out_weight.shape[1]
    tokens_here = stream.shape[1]
    row_start = lax.axis_index("tp") * shard_features
    whole = stream.astype(jnp.float32)
    current = lax.dynamic_slice_in_dim(whole, row_start, shard_features, 0)
    layer_out = stream
    for layer in range(LAYERS):
        both_weights = jnp.concatenate((value_weight[layer], gate_weight[layer]), axis=0)
        if layer == 0:
            projected = norm_project(whole, norm_gain[layer], both_weights)
        else:
            gathered = lax.all_gather(layer_out, "tp", axis=0, tiled=True).astype(jnp.float32)
            projected = norm_project(gathered, norm_gain[layer], both_weights)
        gated = (projected[:shard_channels] * jax.nn.sigmoid(projected[shard_channels:])).astype(
            jnp.bfloat16
        )
        earlier = shifted(gated[:, tokens_here - (K - 1) :], "sp", 1)
        extended = jnp.concatenate((earlier, gated), axis=1).astype(jnp.float32)
        filtered = depthwise(extended, conv_kernel[layer]) + conv_bias[layer][:, None]
        first_sum, square_sum = lax.psum(
            (
                jnp.sum(filtered, axis=0, keepdims=True),
                jnp.sum(filtered * filtered, axis=0, keepdims=True),
            ),
            "tp",
        )
        row_mean = first_sum / total_channels
        centred = filtered - row_mean
        spread = square_sum / total_channels - row_mean * row_mean
        activated = jax.nn.silu(
            centred * lax.rsqrt(spread + epsilon) * channel_gain[layer][:, None]
            + channel_bias[layer][:, None]
        ).astype(jnp.bfloat16)

        def accumulate(total, piece, start, weights=out_weight[layer]):
            weight_cols = lax.dynamic_slice_in_dim(weights, start, piece.shape[0], 1)
            return total + jnp.dot(weight_cols, piece, preferred_element_type=jnp.float32)

        zero_branch = jnp.zeros((shard_features, tokens_here), jnp.float32)
        branch = accumulate(
            zero_branch, lax.all_gather(activated, "tp", axis=0, tiled=True), jnp.int32(0)
        )
        layer_out = (current + branch).astype(jnp.bfloat16)
        current = layer_out.astype(jnp.float32)
    return layer_out


def solution(mesh):
    placed = (
        P(None, ("grp", "sp")),
        P(),
        P(None, "tp", None),
        P(None, "tp", None),
        P(None, "tp", None),
        P(None, "tp"),
        P(None, "tp"),
        P(None, "tp"),
        P(None, "tp", None),
    )
    return jax.shard_map(
        local, mesh=mesh, in_specs=placed, out_specs=P("tp", ("grp", "sp")), check_vma=False
    )
```

profile of v0, /device:TPU:1, one launch (start us, length us, event | category | flops | bytes accessed | tf_op | source)
XLA Modules:
  0.0 148.0 jit_solution(8420381912862414514)
XLA Ops:
  6.5 0.0 all-gather.4.cloned.1.call-start
  6.5 0.9 fusion.83
  7.4 2.4 %multiply_reduce_fusion = f32[320]{0:T(512)S(1)} fusion(bf16[4096,320]{0,1:T(8,128)(2,1)} %param.9), kind=kLoop, calls=%fused_computation.14 | loop fusion | flops 3931840 | bytes 2622720 | tf_op jit(solution)/shard_map/reduce_sum | solution.py:33
  9.8 0.0 copy-start
  9.8 10.3 %slice_bitcast_fusion.2 = (bf16[512,4096]{1,0:T(8,128)(2,1)S(1)}, bf16[512,4096]{1,0:T(8,128)(2,1)}, bf16[512,4096]{1,0:T(8,128)(2,1)}, bf16[512,4096]{1,0:T(8,128)(2,1)S(1)}) fusion(bf16[2,512,4096]{2,1,0:T(8,128)(2,1)} %param.12, bf16[2,512,4096]{2,1,0:T(8,128)(2,1)} %param.11), kind=kLoop, calls=%fused_computation.23 | loop fusion | bytes 33554432 | tf_op jit(solution)/shard_map/squeeze | solution.py:58
  20.0 0.0 copy-done
  20.0 0.0 copy-start.2
  20.0 0.0 copy-start.3
  20.1 0.0 copy-start.4
  20.1 2.9 %fusion = f32[1024,320]{0,1:T(8,128)S(1)} fusion(bf16[512,4096]{1,0:T(8,128)(2,1)S(1)} %get-tuple-element.19, bf16[512,4096]{1,0:T(8,128)(2,1)S(1)} %get-tuple-element.30, f32[4096]{0:T(1024)S(1)} %bitcast.97, f32[320]{0:T(512)S(1)} %add_rsqrt_fusion.1, bf16[4096,320]{0,1:T(8,128)(2,1)S(1)} %copy-done), kind=kOutput, calls=%fused_computation | convolution fusion | flops 2706374656 | bytes 12338432 | tf_op jit(solution)/shard_map/dot_general | solution.py:35
  23.0 0.0 copy-start.5
  23.0 0.0 copy-start.6
  23.0 0.2 fusion.53
  23.2 4.0 %collective-permute-start = (bf16[512,30]{0,1:T(8,128)(2,1)S(1)}, bf16[512,30]{0,1:T(8,128)(2,1)S(1)}, u32[]{:S(2)}, u32[]{:S(2)}) collective-permute-start(bf16[512,30]{0,1:T(8,128)(2,1)S(1)} %slice.94), channel_id=1, source_target_pairs={{0,4},{4,8},{8,12},{1,5},{5,9},{9,13},{2,6},{6,10},{10,14},{3,7},{... | collective-permute-start | bytes 92168 | tf_op jit(solution)/shard_map/ppermute | solution.py:16
  27.3 0.0 copy-done.2
  27.3 0.0 copy-done.3
  27.3 0.0 copy-done.4
  27.3 0.9 collective-permute-done
  28.3 0.1 maximum_bitcast_fusion
  28.4 0.1 reshape.26
  28.5 0.2 copy.17
  28.7 0.1 slice.95
  28.7 0.0 copy-done.5
  28.8 0.0 copy-done.6
  28.8 1.6 %convolution_select_fusion.1 = f32[8,44,512]{2,0,1:T(8,128)S(1)} fusion(bf16[512,1,7,30]{0,2,3,1:T(8,128)(2,1)S(1)} %slice.95, bf16[512,1,8,44]{0,2,3,1:T(8,128)(2,1)S(1)} %copy.17, pred[8,44]{0,1:T(8,128)(4,1)S(1)} %copy-done.6, f32[2,512,31]{1,0,2:T(2,128)S(1)} %copy-done.5), kind=kOutput, calls=%fused_computation.40 | convolution fusion | flops 69042176 | bytes 1396736 | tf_op jit(solution)/shard_map/conv_general_dilated | solution.py:20
  30.3 1.3 copy.18
  31.6 1.2 reshape.30
  32.8 0.2 fusion.67
  33.1 6.5 %all-reduce.1 = (f32[1,320]{1,0:T(1,128)S(1)}, f32[1,320]{1,0:T(1,128)S(1)}) all-reduce(f32[1,320]{1,0:T(1,128)S(1)} %broadcast_in_dim.21, f32[1,320]{1,0:T(1,128)S(1)} %broadcast_in_dim.22), channel_id=1, replica_groups=mesh['grp'=2,'sp'=4,'tp'=4] {'tp'}, use_global_device_ids=true, to_apply=%region_2.0 | all-reduce | flops 640 | bytes 5120 | tf_op jit(solution)/shard_map/psum | solution.py:70
  39.6 1.0 multiply_convert_fusion.3
  40.7 0.0 all-gather.4.cloned.1.call-update
  40.7 0.0 all-gather.6.cloned.1.call-start
  40.7 2.9 %convert_element_type.35 = f32[4096,320]{0,1:T(8,128)} convert(bf16[4096,320]{0,1:T(8,128)(2,1)S(1)} %copy-done) | non-fusion elementwise | flops 1310720 | bytes 7864320 | tf_op jit(solution)/shard_map/convert_element_type | solution.py:54
  43.7 17.9 %all-gather.4.cloned.1.call-done = bf16[2048,320]{0,1:T(8,128)(2,1)} async-done(((bf16[512,320]{0,1:T(8,128)(2,1)}), bf16[2048,320]{0,1:T(8,128)(2,1)}) %all-gather.4.cloned.1.call-update) | async-done | bytes 1310736 | tf_op jit(solution)/shard_map/all_gather | solution.py:91
  61.6 5.4 %fusion.35 = bf16[1024,320]{0,1:T(8,128)(2,1)} fusion(bf16[2048,320]{0,1:T(8,128)(2,1)} %all-gather.4.cloned.1.call-done, bf16[2,1024,2048]{2,1,0:T(8,128)(2,1)} %param.17, f32[4096,320]{0,1:T(8,128)} %convert_element_type.35, s32[]{:T(128)S(6)} %select_n.3), kind=kOutput, calls=%fused_computation.34 | convolution fusion | flops 1342832640 | bytes 7471108 | tf_op jit(solution)/shard_map/dot_general | solution.py:87
  66.9 0.0 all-gather.6.cloned.1.call-update
  67.0 0.2 all-gather.8.cloned.1.call-start
  67.2 25.5 %all-gather.6.cloned.1.call-done = bf16[4096,320]{0,1:T(8,128)(2,1)} async-done(((bf16[1024,320]{0,1:T(8,128)(2,1)}), bf16[4096,320]{0,1:T(8,128)(2,1)}) %all-gather.6.cloned.1.call-update) | async-done | bytes 2621456 | tf_op jit(solution)/shard_map/all_gather | solution.py:62
  92.7 2.3 %fusion.8 = f32[320]{0:T(512)S(1)} fusion(bf16[4096,320]{0,1:T(8,128)(2,1)} %all-gather.6.cloned.1.call-done), kind=kLoop, calls=%fused_computation.10 | loop fusion | flops 3931840 | bytes 2622720 | tf_op jit(solution)/shard_map/reduce_sum | solution.py:33
  95.0 7.1 %fusion.4 = f32[1024,320]{0,1:T(8,128)S(1)} fusion(bf16[512,4096]{1,0:T(8,128)(2,1)} %get-tuple-element.20, bf16[512,4096]{1,0:T(8,128)(2,1)} %get-tuple-element.29, bf16[4096,320]{0,1:T(8,128)(2,1)} %all-gather.6.cloned.1.call-done, f32[4096]{0:T(1024)S(1)} %bitcast.96, f32[320]{0:T(512)S(1)} %add_rsqrt_fusion), kind=kOutput, calls=%fused_computation.4 | convolution fusion | flops 2706374656 | bytes 12338432 | tf_op jit(solution)/shard_map/dot_general | solution.py:35
  102.1 0.2 fusion.54
  102.4 3.1 %collective-permute-start.1 = (bf16[512,30]{0,1:T(8,128)(2,1)S(1)}, bf16[512,30]{0,1:T(8,128)(2,1)S(1)}, u32[]{:S(2)}, u32[]{:S(2)}) collective-permute-start(bf16[512,30]{0,1:T(8,128)(2,1)S(1)} %slice.99), channel_id=1, source_target_pairs={{0,4},{4,8},{8,12},{1,5},{5,9},{9,13},{2,6},{6,10},{10,14},{3,7},{... | collective-permute-start | bytes 92168 | tf_op jit(solution)/shard_map/ppermute | solution.py:16
  105.5 1.0 collective-permute-done.1
  106.5 0.1 maximum_bitcast_fusion.1
  106.6 0.1 reshape.33
  106.7 0.2 copy.20
  106.9 0.1 slice.100
  106.9 1.7 %convolution_select_fusion = f32[8,44,512]{2,0,1:T(8,128)S(1)} fusion(bf16[512,1,7,30]{0,2,3,1:T(8,128)(2,1)S(1)} %slice.100, bf16[512,1,8,44]{0,2,3,1:T(8,128)(2,1)S(1)} %copy.20, pred[8,44]{0,1:T(8,128)(4,1)S(1)} %copy-done.6, f32[2,512,31]{1,0,2:T(2,128)S(1)} %copy-done.5), kind=kOutput, calls=%fused_computation.39 | convolution fusion | flops 69042176 | bytes 1396736 | tf_op jit(solution)/shard_map/conv_general_dilated | solution.py:20
  108.7 0.0 copy-start.1
  108.7 0.4 copy.21
  109.1 0.1 reshape.37
  109.2 0.2 fusion.68
  109.4 6.2 %all-reduce = (f32[1,320]{1,0:T(1,128)S(1)}, f32[1,320]{1,0:T(1,128)S(1)}) all-reduce(f32[1,320]{1,0:T(1,128)S(1)} %broadcast_in_dim.24, f32[1,320]{1,0:T(1,128)S(1)} %broadcast_in_dim.25), channel_id=1, replica_groups=mesh['grp'=2,'sp'=4,'tp'=4] {'tp'}, use_global_device_ids=true, to_apply=%region_7.8 | all-reduce | flops 640 | bytes 5120 | tf_op jit(solution)/shard_map/psum | solution.py:70
  115.6 1.1 multiply_convert_fusion.2
  116.6 0.0 all-gather.8.cloned.1.call-update
  116.7 19.8 %all-gather.8.cloned.1.call-done = bf16[2048,320]{0,1:T(8,128)(2,1)} async-done(((bf16[512,320]{0,1:T(8,128)(2,1)}), bf16[2048,320]{0,1:T(8,128)(2,1)}) %all-gather.8.cloned.1.call-update) | async-done | bytes 1310736 | tf_op jit(solution)/shard_map/all_gather | solution.py:91
  136.5 0.0 copy-done.1
  136.5 5.0 %fusion.38 = bf16[1024,320]{0,1:T(8,128)(2,1)} fusion(bf16[2048,320]{0,1:T(8,128)(2,1)} %all-gather.8.cloned.1.call-done, bf16[2,1024,2048]{2,1,0:T(8,128)(2,1)} %param.17, bf16[1024,320]{0,1:T(8,128)(2,1)S(1)} %copy-done.1), kind=kOutput, calls=%fused_computation.35 | convolution fusion | flops 1343160320 | bytes 6815744 | tf_op jit(solution)/shard_map/dot_general | solution.py:87
  (15 shorter events, 0.2 us)
Async XLA Ops:
  6.5 55.0 %all-gather.4.cloned.1.call-start = ((), (), s32[]{:S(2)}) async-start(), calls=%async_computation | async-start | bytes 1638400 | tf_op jit(solution)/shard_map/all_gather | solution.py:91
  9.8 10.3 %copy-start = (bf16[4096,320]{0,1:T(8,128)(2,1)S(1)}, bf16[4096,320]{0,1:T(8,128)(2,1)}, u32[]{:S(2)}) copy-start(bf16[4096,320]{0,1:T(8,128)(2,1)} %param.9) | copy-start | bytes 7864324
  20.0 7.2 %copy-start.2 = (f32[2,512]{1,0:T(2,128)S(1)}, f32[2,512]{1,0:T(2,128)}, u32[]{:S(2)}) copy-start(f32[2,512]{1,0:T(2,128)} %param.16) | copy-start | bytes 12292
  20.0 7.2 %copy-start.3 = (f32[2,512]{1,0:T(2,128)S(1)}, f32[2,512]{1,0:T(2,128)}, u32[]{:S(2)}) copy-start(f32[2,512]{1,0:T(2,128)} %param.15) | copy-start | bytes 12292
  20.1 7.3 %copy-start.4 = (f32[2,512]{1,0:T(2,128)S(1)}, f32[2,512]{1,0:T(2,128)}, u32[]{:S(2)}) copy-start(f32[2,512]{1,0:T(2,128)} %param.14) | copy-start | bytes 12292
  23.0 5.7 %copy-start.5 = (f32[2,512,31]{1,0,2:T(2,128)S(1)}, f32[2,512,31]{1,0,2:T(2,128)}, u32[]{:S(2)}) copy-start(f32[2,512,31]{1,0,2:T(2,128)} %param.13) | copy-start | bytes 380932
  23.0 5.7 %copy-start.6 = (pred[8,44]{0,1:T(8,128)(4,1)S(1)}, pred[8,44]{0,1:T(8,128)(4,1)}, u32[]{:S(2)}) copy-start(pred[8,44]{0,1:T(8,128)(4,1)} %constant.41) | copy-start | bytes 1060
  23.2 5.0 %collective-permute-start = (bf16[512,30]{0,1:T(8,128)(2,1)S(1)}, bf16[512,30]{0,1:T(8,128)(2,1)S(1)}, u32[]{:S(2)}, u32[]{:S(2)}) collective-permute-start(bf16[512,30]{0,1:T(8,128)(2,1)S(1)} %slice.94), channel_id=1, source_target_pairs={{0,4},{4,8},{8,12},{1,5},{5,9},{9,13},{2,6},{6,10},{10,14},{3,7},{... | collective-permute-start | bytes 92168 | tf_op jit(solution)/shard_map/ppermute | solution.py:16
  40.7 52.0 %all-gather.6.cloned.1.call-start = ((), (), s32[]{:S(2)}) async-start(), calls=%async_computation.1 | async-start | bytes 3276800 | tf_op jit(solution)/shard_map/all_gather | solution.py:62
  67.0 69.5 %all-gather.8.cloned.1.call-start = ((), (), s32[]{:S(2)}) async-start(), calls=%async_computation.2 | async-start | bytes 1638400 | tf_op jit(solution)/shard_map/all_gather | solution.py:91
  102.4 4.1 %collective-permute-start.1 = (bf16[512,30]{0,1:T(8,128)(2,1)S(1)}, bf16[512,30]{0,1:T(8,128)(2,1)S(1)}, u32[]{:S(2)}, u32[]{:S(2)}) collective-permute-start(bf16[512,30]{0,1:T(8,128)(2,1)S(1)} %slice.99), channel_id=1, source_target_pairs={{0,4},{4,8},{8,12},{1,5},{5,9},{9,13},{2,6},{6,10},{10,14},{3,7},{... | collective-permute-start | bytes 92168 | tf_op jit(solution)/shard_map/ppermute | solution.py:16
  108.7 27.8 %copy-start.1 = (bf16[1024,320]{0,1:T(8,128)(2,1)S(1)}, bf16[1024,320]{0,1:T(8,128)(2,1)}, u32[]{:S(2)}) copy-start(bf16[1024,320]{0,1:T(8,128)(2,1)} %fusion.35) | copy-start | bytes 1966084
Sparse Core Ops, SparseCore 0:
  40.8 20.7 all-gather.3
  67.1 25.5 all-gather.5
  116.8 19.6 all-gather.7
where the time goes:
time: 149 us; the launch traced here: 148 us
  waiting for transfers between devices  65.1 us (44%)
  matrix products  23.7 us (16%)
  local copies, waits for them, and re-layouts  14.9 us (10%)
  between operations  13.4 us (9%)
  blocking collectives  12.7 us (9%)
  other arithmetic  10.7 us (7%)
  starting transfers between devices  7.4 us (5%)
    all_gather x2, waiting for transfers between devices, local(): lax.all_gather(activated, 'tp', axis=0, tiled=True)  37.7 us
    all_gather x1, waiting for transfers between devices, local(): lax.all_gather(layer_out, 'tp', axis=0, tiled=True).astype(jnp.float32)  25.5 us
    psum x2, blocking collectives, local(): lax.psum((jnp.sum(filtered, axis=0, keepdims=True), jnp.sum(filtered * fi...  12.7 us
    dot_general x2, matrix products, accumulate(): jnp.dot(weight_cols, piece, preferred_element_type=jnp.float32)  10.3 us
    squeeze x1, local copies, waits for them, and re-layouts, local(): gate_weight[layer]  10.3 us
    dot_general x2, matrix products, norm_project(): return jnp.dot(weights, normed, preferred_element_type=jnp.float32)  10.1 us
    ppermute x2, starting transfers between devices, shifted(): lax.ppermute(value, axis, [(source, source + steps) for source in range(i...  7.13 us
    reduce_sum x2, other arithmetic, norm_project(): jnp.mean(whole * whole, axis=0, keepdims=True) + epsilon  4.7 us
  transfers between devices with their start and end apart: 5, of which 5 were waited for; matrix products, arithmetic and copies ran while one was open for 2% of the time, Pallas kernels for 0%

commit v1 on v0

--- a/solution.py
+++ b/solution.py
@@ -1,6 +1,10 @@
+import functools
+
 import jax
 import jax.numpy as jnp
 from jax import lax
+from jax.experimental import pallas as pl
+from jax.experimental.pallas import tpu as pltpu
 from jax.sharding import PartitionSpec as P
 
 K = 31
@@ -95,6 +99,438 @@
     return layer_out
 
 
+MESH = pl.DeviceIdType.MESH
+LANES = 128
+CHUNK = 256
+HALO = 32
+ROWS = 64
+CORES = 2
+WEIGHT_PIECES = 4
+
+
+def dot_nt(left, right):
+    return lax.dot_general(
+        left, right, (((1,), (1,)), ((), ())), preferred_element_type=jnp.float32
+    )
+
+
+def kernel(
+    n_tp,
+    n_sp,
+    x_ref,
+    gain_ref,
+    param_ref,
+    wv_ref,
+    wg_ref,
+    ow_ref,
+    out_ref,
+    wp,
+    wo,
+    xg,
+    ext,
+    filt,
+    part,
+    column,
+    halo_out,
+    halo_in,
+    stat,
+    ag,
+    sg,
+    accp,
+    acco,
+    res,
+    wp_sem,
+    wo_sem,
+    halo_send,
+    halo_recv,
+    stat_send,
+    stat_recv,
+    y_send,
+    y_recv,
+    f_send,
+    f_recv,
+):
+    tokens, width = x_ref.shape
+    chans = wv_ref.shape[1]
+    feats = ow_ref.shape[1]
+    total_chans = chans * n_tp
+    n_y = n_tp // CORES
+    piece = width // WEIGHT_PIECES
+    padded = part.shape[1]
+    me = lax.axis_index("tp")
+    sp = lax.axis_index("sp")
+    my_y, core = me // CORES, me % CORES
+    sibling = my_y * CORES + (1 - core)
+
+    def tp_id(index):
+        return {"tp": index}
+
+    barrier = pltpu.get_barrier_semaphore()
+    for step in range(1, n_tp):
+        pl.semaphore_signal(
+            barrier, inc=1, device_id=tp_id(lax.rem(me + step, n_tp)), device_id_type=MESH
+        )
+
+    @pl.when(sp > 0)
+    def _():
+        pl.semaphore_signal(barrier, inc=1, device_id={"sp": sp - 1}, device_id_type=MESH)
+
+    @pl.when(sp < n_sp - 1)
+    def _():
+        pl.semaphore_signal(barrier, inc=1, device_id={"sp": sp + 1}, device_id_type=MESH)
+
+    def proj_copies(layer, index):
+        cols = pl.ds(index * piece, piece)
+        return [
+            pltpu.make_async_copy(
+                ref.at[layer, :, cols], wp.at[layer, half, :, cols], wp_sem.at[layer, index]
+            )
+            for half, ref in enumerate((wv_ref, wg_ref))
+        ]
+
+    def out_copy(layer):
+        return pltpu.make_async_copy(ow_ref.at[layer], wo.at[layer], wo_sem.at[layer])
+
+    for layer in range(LAYERS):
+        for index in range(WEIGHT_PIECES):
+            for copy in proj_copies(layer, index):
+                copy.start()
+        out_copy(layer).start()
+
+    def prepare(layer, read, first_col, cols, first):
+        gains = gain_ref[layer : layer + 1, pl.ds(first_col, cols)]
+
+        @pl.loop(0, tokens // ROWS)
+        def _(block):
+            rows = pl.ds(pl.multiple_of(block * ROWS, ROWS), ROWS)
+            squares = jnp.zeros((ROWS, LANES), jnp.float32)
+            if not first:
+                squares = part[0, rows, :]
+            for lane in range(cols // LANES):
+                here = slice(lane * LANES, (lane + 1) * LANES)
+                values = read(rows, here).astype(jnp.float32)
+                squares = squares + values * values
+                xg[rows, here] = (values * gains[:, here]).astype(jnp.bfloat16)
+            part[0, rows, :] = squares
+
+    def project(layer, first_col, cols, first):
+        for half in range(2):
+            held = slice(half * chans, (half + 1) * chans)
+            product = dot_nt(xg[:, :cols], wp[layer, half, :, pl.ds(first_col, cols)])
+            if first:
+                accp[:, held] = product
+            else:
+                accp[:, held] += product
+
+    pending = []
+
+    def remote(source, target, send, recv, device):
+        copy = pltpu.make_async_remote_copy(
+            src_ref=source,
+            dst_ref=target,
+            send_sem=send,
+            recv_sem=recv,
+            device_id=tp_id(device),
+            device_id_type=MESH,
+        )
+        return copy
+
+    def y_copy(phase, buf, step, chunk, owner):
+        target = lax.rem(my_y + step, n_y) * CORES + core
+        ref = buf.at[owner, chunk]
+        return remote(
+            ref, ref, y_send.at[phase, step, chunk], y_recv.at[phase, step, chunk], target
+        )
+
+    def f_copy(phase, buf, step, chunk, owner):
+        ref = buf.at[owner, chunk]
+        return remote(
+            ref, ref, f_send.at[phase, step, chunk], f_recv.at[phase, step, chunk], sibling
+        )
+
+    def send_own(phase, buf, chunk):
+        for step in range(1, n_y):
+            copy = y_copy(phase, buf, step, chunk, me)
+            copy.start()
+            pending.append(copy)
+        copy = f_copy(phase, buf, 0, chunk, me)
+        copy.start()
+        pending.append(copy)
+
+    def gather(phase, buf, chunks, use):
+        for chunk in range(chunks):
+            use(me, chunk, chunk == 0)
+        for chunk in range(chunks):
+            f_copy(phase, buf, 0, chunk, sibling).wait_recv()
+            use(sibling, chunk, False)
+        for step in range(1, n_y):
+            origin = lax.rem(my_y + n_y - step, n_y) * CORES
+            for chunk in range(chunks):
+                y_copy(phase, buf, step, chunk, origin + core).wait_recv()
+                copy = f_copy(phase, buf, step, chunk, origin + core)
+                copy.start()
+                pending.append(copy)
+                use(origin + core, chunk, False)
+                f_copy(phase, buf, step, chunk, origin + 1 - core).wait_recv()
+                use(origin + 1 - core, chunk, False)
+
+    def gate(layer, first_row, count):
+        rows = pl.ds(first_row, count)
+        scaling = lax.rsqrt(
+            jnp.sum(part[0, rows, :], axis=1, keepdims=True) / width + epsilon
+        )
+        value = accp[rows, :chans] * scaling
+        gates = accp[rows, chans:] * scaling
+        gated = (value * jax.nn.sigmoid(gates)).astype(jnp.bfloat16)
+        widened = gated.astype(jnp.float32)
+        for lane in range(chans // LANES):
+            ext[lane, pl.ds(first_row + HALO, count), :] = widened[
+                :, lane * LANES : (lane + 1) * LANES
+            ]
+        return gated
+
+    def convolve(layer, blocks):
+        @pl.loop(0, chans // LANES)
+        def _(lane):
+            here = pl.ds(pl.multiple_of(lane * LANES, LANES), LANES)
+            bias = jnp.broadcast_to(param_ref[layer, K : K + 1, here], (ROWS, LANES))
+            for block in blocks:
+                first_row = block * ROWS
+                rows = slice(first_row, first_row + ROWS)
+                total = bias
+                for tap in range(K):
+                    start = first_row + HALO - K + 1 + tap
+                    window = ext[lane, start : start + ROWS, :]
+                    total = total + window * param_ref[layer, tap : tap + 1, here]
+                filt[rows, here] = total
+                part[0, rows, :] += total
+                part[1, rows, :] += total * total
+
+    for layer in range(LAYERS):
+        if layer == 0:
+            for index in range(WEIGHT_PIECES):
+                start = index * piece
+                prepare(
+                    layer,
+                    lambda rows, here, start=start: x_ref[
+                        rows, start + here.start : start + here.stop
+                    ],
+                    start,
+                    piece,
+                    index == 0,
+                )
+                for copy in proj_copies(layer, index):
+                    copy.wait()
+                project(layer, start, piece, index == 0)
+            res[...] = x_ref[:, pl.ds(pl.multiple_of(me * feats, LANES), feats)].astype(jnp.float32)
+            pl.semaphore_wait(
+                barrier,
+                n_tp - 1 + jnp.where(sp > 0, 1, 0) + jnp.where(sp < n_sp - 1, 1, 0),
+            )
+        else:
+            for index in range(WEIGHT_PIECES):
+                for copy in proj_copies(layer, index):
+                    copy.wait()
+
+            def use_stream(owner, chunk, first):
+                start = pl.multiple_of(owner * feats + chunk * CHUNK, LANES)
+                prepare(
+                    layer,
+                    lambda rows, here: sg[owner, chunk, rows, here],
+                    start,
+                    CHUNK,
+                    first,
+                )
+                project(layer, start, CHUNK, first)
+
+            gather(1, sg, feats // CHUNK, use_stream)
+
+        last_rows = tokens - HALO
+        halo_out[layer] = gate(layer, last_rows, HALO)
+        to_next = pltpu.make_async_remote_copy(
+            src_ref=halo_out.at[layer],
+            dst_ref=halo_in.at[layer],
+            send_sem=halo_send.at[layer],
+            recv_sem=halo_recv.at[layer],
+            device_id={"sp": lax.rem(sp + 1, n_sp)},
+            device_id_type=MESH,
+        )
+
+        @pl.when(sp < n_sp - 1)
+        def _():
+            to_next.start()
+
+        @pl.loop(0, last_rows // HALO)
+        def _(block):
+            gate(layer, pl.multiple_of(block * HALO, HALO), HALO)
+
+        part[...] = jnp.zeros(part.shape, jnp.float32)
+        convolve(layer, range(1, tokens // ROWS))
+
+        @pl.when(sp > 0)
+        def _():
+            to_next.wait_recv()
+            for lane in range(chans // LANES):
+                ext[lane, :HALO, :] = halo_in[
+                    layer, :, lane * LANES : (lane + 1) * LANES
+                ].astype(jnp.float32)
+
+        @pl.when(sp == 0)
+        def _():
+            ext[:, :HALO, :] = jnp.zeros((chans // LANES, HALO, LANES), jnp.float32)
+
+        convolve(layer, range(1))
+        first_row = jnp.sum(jnp.transpose(part[0]), axis=0, keepdims=True)
+        square_row = jnp.sum(jnp.transpose(part[1]), axis=0, keepdims=True)
+        row_index = lax.broadcasted_iota(jnp.int32, (8, padded), 0)
+        stat[layer, me] = jnp.where(row_index == 0, first_row, square_row)
+        stat_copies = []
+        for step in range(1, n_tp):
+            copy = remote(
+                stat.at[layer, me],
+                stat.at[layer, me],
+                stat_send.at[layer, step],
+                stat_recv.at[layer, step],
+                lax.rem(me + step, n_tp),
+            )
+            copy.start()
+            pending.append(copy)
+            stat_copies.append(copy)
+        for step in range(1, n_tp):
+            origin = lax.rem(me + n_tp - step, n_tp)
+            remote(
+                stat.at[layer, origin],
+                stat.at[layer, origin],
+                stat_send.at[layer, step],
+                stat_recv.at[layer, step],
+                origin,
+            ).wait_recv()
+        totals = jnp.sum(stat[layer], axis=0) / total_chans
+        mean_row = totals[0:1]
+        rstd_row = lax.rsqrt(totals[1:2] - mean_row * mean_row + epsilon)
+        column[0] = jnp.transpose(jnp.broadcast_to(mean_row, (LANES, padded)))
+        column[1] = jnp.transpose(jnp.broadcast_to(rstd_row, (LANES, padded)))
+
+        phase = 0 if layer == 0 else 2
+        for chunk in range(chans // CHUNK):
+
+            @pl.loop(0, tokens // ROWS)
+            def _(block):
+                rows = pl.ds(pl.multiple_of(block * ROWS, ROWS), ROWS)
+                for lane in range(CHUNK // LANES):
+                    here = slice(chunk * CHUNK + lane * LANES, chunk * CHUNK + (lane + 1) * LANES)
+                    values = (filt[rows, here] - column[0, rows, :]) * column[1, rows, :]
+                    values = (
+                        values * param_ref[layer, K + 1 : K + 2, here]
+                        + param_ref[layer, K + 2 : K + 3, here]
+                    )
+                    ag[layer, me, chunk, rows, lane * LANES : (lane + 1) * LANES] = (
+                        jax.nn.silu(values).astype(jnp.bfloat16)
+                    )
+
+            send_own(phase, ag.at[layer], chunk)
+
+        out_copy(layer).wait()
+
+        def use_activated(owner, chunk, first):
+            start = pl.multiple_of(owner * chans + chunk * CHUNK, LANES)
+            product = dot_nt(ag[layer, owner, chunk], wo[layer, :, pl.ds(start, CHUNK)])
+            if first:
+                acco[...] = res[...] + product
+            else:
+                acco[...] += product
+
+        gather(phase, ag.at[layer], chans // CHUNK, use_activated)
+
+        if layer < LAYERS - 1:
+            for chunk in range(feats // CHUNK):
+                here = slice(chunk * CHUNK, (chunk + 1) * CHUNK)
+                rounded = acco[:, here].astype(jnp.bfloat16)
+                sg[me, chunk] = rounded
+                send_own(1, sg, chunk)
+                res[:, here] = rounded.astype(jnp.float32)
+        else:
+            out_ref[...] = acco[...].astype(jnp.bfloat16)
+
+        @pl.when(sp < n_sp - 1)
+        def _():
+            to_next.wait_send()
+
+    for copy in pending:
+        copy.wait_send()
+
+
+def fused(mesh, stream, norm_gain, value_weight, gate_weight, conv_kernel, conv_bias,
+          channel_gain, channel_bias, out_weight):
+    n_tp, n_sp = mesh.shape["tp"], mesh.shape["sp"]
+    width, tokens = stream.shape
+    chans, feats = value_weight.shape[1], out_weight.shape[1]
+    fits = (
+        n_tp % CORES == 0
+        and chans % CHUNK == 0
+        and feats % CHUNK == 0
+        and width % (WEIGHT_PIECES * CHUNK) == 0
+        and tokens % ROWS == 0
+        and n_tp <= 8
+    )
+    if not fits:
+        return local(stream, norm_gain, value_weight, gate_weight, conv_kernel, conv_bias,
+                     channel_gain, channel_bias, out_weight)
+    padded = -(-tokens // LANES) * LANES
+    n_y = n_tp // CORES
+    n_a, n_f = chans // CHUNK, feats // CHUNK
+    most = max(n_a, n_f)
+    params = jnp.concatenate(
+        (
+            jnp.swapaxes(conv_kernel, 1, 2),
+            conv_bias[:, None],
+            channel_gain[:, None],
+            channel_bias[:, None],
+        ),
+        axis=1,
+    )
+    f32, bf16 = jnp.float32, jnp.bfloat16
+    vmem = pl.BlockSpec(memory_space=pltpu.VMEM)
+    anyspace = pl.BlockSpec(memory_space=pl.ANY)
+    out = pl.pallas_call(
+        functools.partial(kernel, n_tp, n_sp),
+        out_shape=jax.ShapeDtypeStruct((tokens, feats), bf16),
+        in_specs=[vmem, vmem, vmem, anyspace, anyspace, anyspace],
+        out_specs=vmem,
+        scratch_shapes=[
+            pltpu.VMEM((LAYERS, 2, chans, width), bf16),
+            pltpu.VMEM((LAYERS, feats, chans * n_tp), bf16),
+            pltpu.VMEM((tokens, width // WEIGHT_PIECES), bf16),
+            pltpu.VMEM((chans // LANES, HALO + tokens, LANES), f32),
+            pltpu.VMEM((tokens, chans), f32),
+            pltpu.VMEM((2, padded, LANES), f32),
+            pltpu.VMEM((2, padded, LANES), f32),
+            pltpu.VMEM((LAYERS, HALO, chans), bf16),
+            pltpu.VMEM((LAYERS, HALO, chans), bf16),
+            pltpu.VMEM((LAYERS, n_tp, 8, padded), f32),
+            pltpu.VMEM((LAYERS, n_tp, n_a, tokens, CHUNK), bf16),
+            pltpu.VMEM((n_tp, n_f, tokens, CHUNK), bf16),
+            pltpu.VMEM((tokens, 2 * chans), f32),
+            pltpu.VMEM((tokens, feats), f32),
+            pltpu.VMEM((tokens, feats), f32),
+            pltpu.SemaphoreType.DMA((LAYERS, WEIGHT_PIECES)),
+            pltpu.SemaphoreType.DMA((LAYERS,)),
+            pltpu.SemaphoreType.DMA((LAYERS,)),
+            pltpu.SemaphoreType.DMA((LAYERS,)),
+            pltpu.SemaphoreType.DMA((LAYERS, n_tp)),
+            pltpu.SemaphoreType.DMA((LAYERS, n_tp)),
+            pltpu.SemaphoreType.DMA((3, n_y, most)),
+            pltpu.SemaphoreType.DMA((3, n_y, most)),
+            pltpu.SemaphoreType.DMA((3, n_y, most)),
+            pltpu.SemaphoreType.DMA((3, n_y, most)),
+        ],
+        compiler_params=pltpu.CompilerParams(
+            collective_id=0, has_side_effects=True, vmem_limit_bytes=60 * 1024 * 1024
+        ),
+    )(stream.T, norm_gain, params, value_weight, gate_weight, out_weight)
+    return out.T
+
+
 def solution(mesh):
     placed = (
         P(None, ("grp", "sp")),
@@ -108,5 +544,5 @@
         P(None, "tp", None),
     )
     return jax.shard_map(
-        local, mesh=mesh, in_specs=placed, out_specs=P("tp", ("grp", "sp")), check_vma=False
+        functools.partial(fused, mesh), mesh=mesh, in_specs=placed, out_specs=P("tp", ("grp", "sp")), check_vma=False
     )

time: 149 us -> 66.5 us (0.45)
  waiting for transfers between devices: 65.1 us -> 0 us
  Pallas kernels: 0 us -> 60.5 us
  matrix products: 23.7 us -> 0 us
  between operations: 13.4 us -> 0.01 us
  blocking collectives: 12.7 us -> 0 us
  other arithmetic: 10.7 us -> 0.69 us
  local copies, waits for them, and re-layouts: 14.9 us -> 4.96 us
  starting transfers between devices: 7.4 us -> 0 us
    all_gather x3 -> x0, waiting for transfers between devices: 63.1 us -> none  [the longest x2 37.7 us: local(): lax.all_gather(activated, 'tp', axis=0, tiled=True)]
    pallas_call x0 -> x1, Pallas kernels: none -> 60.5 us  [fused(): pl.pallas_call(functools.partial(kernel, n_tp, n_sp), out_shape=jax.Shape...]
    dot_general x4 -> x0, matrix products: 20.4 us -> none  [the longest x2 10.3 us: accumulate(): jnp.dot(weight_cols, piece, preferred_element_type=jnp.float32)]
    psum x2 -> x0, blocking collectives: 12.7 us -> none  [local(): lax.psum((jnp.sum(filtered, axis=0, keepdims=True), jnp.sum(filtered * fi...]
    squeeze x1 -> x0, local copies, waits for them, and re-layouts: 10.3 us -> none  [local(): gate_weight[layer]]
    ppermute x2 -> x0, starting transfers between devices: 7.13 us -> none  [shifted(): lax.ppermute(value, axis, [(source, source + steps) for source in range(i...]
    convert_element_type x5 -> x0, other arithmetic: 5.39 us -> none  [the longest x1 2.94 us: local(): whole = stream.astype(jnp.float32)]
    reduce_sum x4 -> x0, other arithmetic: 5.09 us -> none  [the longest x2 4.7 us: norm_project(): jnp.mean(whole * whole, axis=0, keepdims=True) + epsilon]
  transfers between devices with their start and end apart: 5 -> 0, of which waited for: 5 -> 0; matrix products, arithmetic and copies ran while one was open for 2% -> 0% of each run, Pallas kernels for 0% -> 0%
where the time goes in v1:
time: 66.5 us; the launch traced here: 66.2 us
  Pallas kernels  60.5 us (91%)
  local copies, waits for them, and re-layouts  4.96 us (7%)
  other arithmetic  0.69 us (1%)
    pallas_call x1, Pallas kernels, fused(): pl.pallas_call(functools.partial(kernel, n_tp, n_sp), out_shape=jax.Shape...  60.5 us
    unnamed x2, local copies, waits for them, and re-layouts  2.89 us

profile of v1, /device:TPU:1, one launch (start us, length us, event | category | flops | bytes accessed | tf_op | source)
XLA Modules:
  0.0 66.2 jit_solution(5049454974330739260)
XLA Ops:
  0.0 0.7 %broadcast_in_dim.9 = f32[2,1,512]{2,1,0:T(1,128)S(1)} reshape(f32[2,512]{1,0:T(2,128)} %param.14) | data formatting | bytes 8192 | tf_op jit(solution)/shard_map/broadcast_in_dim | solution.py:486
  0.7 0.7 %broadcast_in_dim.10 = f32[2,1,512]{2,1,0:T(1,128)S(1)} reshape(f32[2,512]{1,0:T(2,128)} %param.15) | data formatting | bytes 8192 | tf_op jit(solution)/shard_map/broadcast_in_dim | solution.py:487
  1.4 0.7 %broadcast_in_dim.11 = f32[2,1,512]{2,1,0:T(1,128)S(1)} reshape(f32[2,512]{1,0:T(2,128)} %param.16) | data formatting | bytes 8192 | tf_op jit(solution)/shard_map/broadcast_in_dim | solution.py:488
  2.1 0.9 %copy.12 = f32[2,512,31]{1,2,0:T(8,128)S(1)} copy(f32[2,512,31]{1,0,2:T(2,128)} %param.13) | data formatting | bytes 253952 | tf_op args[4]
  3.0 0.7 %pad_maximum_fusion.param_ref = f32[2,34,512]{2,1,0:T(8,128)} fusion(f32[2,1,512]{2,1,0:T(1,128)S(1)} %broadcast_in_dim.11, f32[2,1,512]{2,1,0:T(1,128)S(1)} %broadcast_in_dim.10, f32[2,1,512]{2,1,0:T(1,128)S(1)} %broadcast_in_dim.9, f32[2,31,512]{2,1,0:T(8,128)S(1)} %bitcast.7), kind=kLoop, calls=%fused_computation | loop fusion | flops 104448 | bytes 278528 | tf_op jit(solution)/shard_map/concatenate | solution.py:483
  3.7 60.5 %shard_map.91 = bf16[320,1024]{1,0:T(8,128)(2,1)} custom-call(bf16[320,4096]{1,0:T(8,128)(2,1)} %bitcast.6, f32[2,4096]{1,0:T(2,128)} %gain_ref.1, f32[2,34,512]{2,1,0:T(8,128)} %pad_maximum_fusion.param_ref, bf16[2,512,4096]{2,1,0:T(8,128)(2,1)} %wv_ref.1, bf16[2,512,4096]{2,1,0:T(8,128)(2,1)} %wg_ref.1, bf16[2,1024,2048]{2,1,0:T(8,128)(2,1)} %ow_ref.1), custom_call_target="tpu_custom_call" | custom-call | tf_op jit(solution)/shard_map/pallas_call | solution.py:495
  64.2 2.0 %copy.14 = bf16[1024,320]{0,1:T(8,128)(2,1)} copy(bf16[1024,320]{0,1:T(8,128)(2,1)} %bitcast.5) | data formatting | bytes 1310720

commit v2 on v1

v2 whole, which is shorter than its diff:
```python
import functools

import jax
import jax.numpy as jnp
from jax import lax
from jax.experimental import pallas as pl
from jax.experimental.pallas import tpu as pltpu
from jax.sharding import PartitionSpec as P

K = 31
LAYERS = 2


epsilon = 1e-06


def shifted(value, axis, steps):
    count = lax.axis_size(axis)
    initial, last = (max(0, -steps), min(count, count - steps))
    return lax.ppermute(value, axis, [(source, source + steps) for source in range(initial, last)])


def depthwise(signal, kernel):
    out = lax.conv_general_dilated(
        signal[None],
        kernel[:, None, :],
        (1,),
        [(0, 0)],
        dimension_numbers=("NCW", "OIW", "NCW"),
        feature_group_count=kernel.shape[0],
        precision=lax.Precision.HIGHEST,
    )
    return out[0]


def norm_project(whole, gain, weights):
    scaling = lax.rsqrt(jnp.mean(whole * whole, axis=0, keepdims=True) + epsilon)
    normed = (whole * scaling * gain[:, None]).astype(jnp.bfloat16)
    return jnp.dot(weights, normed, preferred_element_type=jnp.float32)


def local(
    stream,
    norm_gain,
    value_weight,
    gate_weight,
    conv_kernel,
    conv_bias,
    channel_gain,
    channel_bias,
    out_weight,
):
    shard_channels = value_weight.shape[1]
    total_channels = shard_channels * lax.axis_size("tp")
    shard_features = out_weight.shape[1]
    tokens_here = stream.shape[1]
    row_start = lax.axis_index("tp") * shard_features
    whole = stream.astype(jnp.float32)
    current = lax.dynamic_slice_in_dim(whole, row_start, shard_features, 0)
    layer_out = stream
    for layer in range(LAYERS):
        both_weights = jnp.concatenate((value_weight[layer], gate_weight[layer]), axis=0)
        if layer == 0:
            projected = norm_project(whole, norm_gain[layer], both_weights)
        else:
            gathered = lax.all_gather(layer_out, "tp", axis=0, tiled=True).astype(jnp.float32)
            projected = norm_project(gathered, norm_gain[layer], both_weights)
        gated = (projected[:shard_channels] * jax.nn.sigmoid(projected[shard_channels:])).astype(
            jnp.bfloat16
        )
        earlier = shifted(gated[:, tokens_here - (K - 1) :], "sp", 1)
        extended = jnp.concatenate((earlier, gated), axis=1).astype(jnp.float32)
        filtered = depthwise(extended, conv_kernel[layer]) + conv_bias[layer][:, None]
        first_sum, square_sum = lax.psum(
            (
                jnp.sum(filtered, axis=0, keepdims=True),
                jnp.sum(filtered * filtered, axis=0, keepdims=True),
            ),
            "tp",
        )
        row_mean = first_sum / total_channels
        centred = filtered - row_mean
        spread = square_sum / total_channels - row_mean * row_mean
        activated = jax.nn.silu(
            centred * lax.rsqrt(spread + epsilon) * channel_gain[layer][:, None]
            + channel_bias[layer][:, None]
        ).astype(jnp.bfloat16)

        def accumulate(total, piece, start, weights=out_weight[layer]):
            weight_cols = lax.dynamic_slice_in_dim(weights, start, piece.shape[0], 1)
            return total + jnp.dot(weight_cols, piece, preferred_element_type=jnp.float32)

        zero_branch = jnp.zeros((shard_features, tokens_here), jnp.float32)
        branch = accumulate(
            zero_branch, lax.all_gather(activated, "tp", axis=0, tiled=True), jnp.int32(0)
        )
        layer_out = (current + branch).astype(jnp.bfloat16)
        current = layer_out.astype(jnp.float32)
    return layer_out


MESH = pl.DeviceIdType.MESH
LANES = 128
CHUNK = 256
HALO = 32
ROWS = 64
CORES = 2
WEIGHT_PIECES = 4


def dot_nt(left, right):
    return lax.dot_general(
        left, right, (((1,), (1,)), ((), ())), preferred_element_type=jnp.float32
    )


def kernel(
    n_tp,
    n_sp,
    x_ref,
    gain_ref,
    taps_ref,
    bias_ref,
    chan_gain_ref,
    chan_bias_ref,
    wv_ref,
    wg_ref,
    ow_ref,
    out_ref,
    wp,
    wo,
    xg,
    ext,
    filt,
    taps,
    norm_squares,
    part,
    column,
    halo_out,
    halo_in,
    stat,
    ag,
    sg,
    accp,
    acco,
    res,
    wp_sem,
    wo_sem,
    halo_send,
    halo_recv,
    stat_send,
    stat_recv,
    y_send,
    y_recv,
    f_send,
    f_recv,
):
    tokens, width = x_ref.shape
    chans = wv_ref.shape[1]
    feats = ow_ref.shape[1]
    total_chans = chans * n_tp
    n_y = n_tp // CORES
    piece = width // WEIGHT_PIECES
    padded = part.shape[2]
    split = (tokens // 2 - HALO) // HALO * HALO
    spans = (
        ((split, tokens), (0, split)),
        ((split + HALO, tokens), (0, split + HALO)),
    )
    me = lax.axis_index("tp")
    sp = lax.axis_index("sp")
    my_y, core = me // CORES, me % CORES
    sibling = my_y * CORES + (1 - core)

    def tp_id(index):
        return {"tp": index}

    barrier = pltpu.get_barrier_semaphore()
    for step in range(1, n_tp):
        pl.semaphore_signal(
            barrier, inc=1, device_id=tp_id(lax.rem(me + step, n_tp)), device_id_type=MESH
        )

    @pl.when(sp > 0)
    def _():
        pl.semaphore_signal(barrier, inc=1, device_id={"sp": sp - 1}, device_id_type=MESH)

    @pl.when(sp < n_sp - 1)
    def _():
        pl.semaphore_signal(barrier, inc=1, device_id={"sp": sp + 1}, device_id_type=MESH)

    def proj_copies(layer, index):
        cols = pl.ds(index * piece, piece)
        return [
            pltpu.make_async_copy(
                ref.at[layer, :, cols], wp.at[layer, half, :, cols], wp_sem.at[layer, index]
            )
            for half, ref in enumerate((wv_ref, wg_ref))
        ]

    def out_copy(layer):
        return pltpu.make_async_copy(ow_ref.at[layer], wo.at[layer], wo_sem.at[layer])

    for layer in range(LAYERS):
        for index in range(WEIGHT_PIECES):
            for copy in proj_copies(layer, index):
                copy.start()
        out_copy(layer).start()

    for layer in range(LAYERS):
        taps[layer] = jnp.transpose(taps_ref[layer])

    def prepare(layer, read, first_col, cols, span, at, first):
        gains = gain_ref[layer : layer + 1, pl.ds(first_col, cols)]

        @pl.loop(0, (span[1] - span[0]) // ROWS)
        def _(block):
            rows = pl.ds(pl.multiple_of(span[0] + block * ROWS, HALO), ROWS)
            squares = jnp.zeros((ROWS, LANES), jnp.float32)
            if not first:
                squares = norm_squares[rows, :]
            for lane in range(cols // LANES):
                here = slice(lane * LANES, (lane + 1) * LANES)
                values = read(rows, here).astype(jnp.float32)
                squares = squares + values * values
                xg[rows, at + here.start : at + here.stop] = (values * gains[:, here]).astype(
                    jnp.bfloat16
                )
            norm_squares[rows, :] = squares

    def project(layer, first_col, cols, span, first):
        rows = slice(*span)
        for half in range(2):
            held = slice(half * chans, (half + 1) * chans)
            product = dot_nt(xg[rows, :cols], wp[layer, half, :, pl.ds(first_col, cols)])
            if first:
                accp[rows, held] = product
            else:
                accp[rows, held] += product

    pending = []

    def remote(source, target, send, recv, device):
        copy = pltpu.make_async_remote_copy(
            src_ref=source,
            dst_ref=target,
            send_sem=send,
            recv_sem=recv,
            device_id=tp_id(device),
            device_id_type=MESH,
        )
        return copy

    def y_copy(phase, buf, step, chunk, owner, rows):
        target = lax.rem(my_y + step, n_y) * CORES + core
        ref = buf.at[owner, chunk, rows]
        return remote(
            ref, ref, y_send.at[phase, step, chunk], y_recv.at[phase, step, chunk], target
        )

    def f_copy(phase, buf, step, chunk, owner, rows):
        ref = buf.at[owner, chunk, rows]
        return remote(
            ref, ref, f_send.at[phase, step, chunk], f_recv.at[phase, step, chunk], sibling
        )

    def send_own(phase, buf, chunk, span):
        rows = pl.ds(span[0], span[1] - span[0])
        for step in range(1, n_y):
            copy = y_copy(phase, buf, step, chunk, me, rows)
            copy.start()
            pending.append(copy)
        copy = f_copy(phase, buf, 0, chunk, me, rows)
        copy.start()
        pending.append(copy)

    def near(phase, buf, chunks, span, use):
        rows = pl.ds(span[0], span[1] - span[0])
        use(me, range(chunks), span, True)
        for chunk in range(chunks):
            f_copy(phase, buf, 0, chunk, sibling, rows).wait_recv()
        use(sibling, range(chunks), span, False)

    def far(phase, buf, chunks, span, use):
        rows = pl.ds(span[0], span[1] - span[0])
        for step in range(1, n_y):
            origin = lax.rem(my_y + n_y - step, n_y) * CORES
            for chunk in range(chunks):
                y_copy(phase, buf, step, chunk, origin + core, rows).wait_recv()
                copy = f_copy(phase, buf, step, chunk, origin + core, rows)
                copy.start()
                pending.append(copy)
                use(origin + core, (chunk,), span, False)
                f_copy(phase, buf, step, chunk, origin + 1 - core, rows).wait_recv()
                use(origin + 1 - core, (chunk,), span, False)

    def gate(first_row, count):
        rows = pl.ds(first_row, count)
        scaling = lax.rsqrt(
            jnp.sum(norm_squares[rows, :], axis=1, keepdims=True) / width + epsilon
        )
        value = accp[rows, :chans] * scaling
        gates = accp[rows, chans:] * scaling
        gated = (value * jax.nn.sigmoid(gates)).astype(jnp.bfloat16)
        widened = gated.astype(jnp.float32)
        for lane in range(chans // LANES):
            ext[lane, pl.ds(first_row + HALO, count), :] = widened[
                :, lane * LANES : (lane + 1) * LANES
            ]
        return gated

    def gate_rows(start, stop):
        @pl.loop(0, (stop - start) // HALO)
        def _(block):
            gate(pl.multiple_of(start + block * HALO, HALO), HALO)

    def halo_copy(layer):
        return pltpu.make_async_remote_copy(
            src_ref=halo_out.at[layer],
            dst_ref=halo_in.at[layer],
            send_sem=halo_send.at[layer],
            recv_sem=halo_recv.at[layer],
            device_id={"sp": lax.rem(sp + 1, n_sp)},
            device_id_type=MESH,
        )

    def send_halo(layer):
        halo_out[layer] = gate(tokens - HALO, HALO)

        @pl.when(sp < n_sp - 1)
        def _():
            halo_copy(layer).start()

    def receive_halo(layer):
        @pl.when(sp > 0)
        def _():
            halo_copy(layer).wait_recv()
            for lane in range(chans // LANES):
                ext[lane, :HALO, :] = halo_in[
                    layer, :, lane * LANES : (lane + 1) * LANES
                ].astype(jnp.float32)

        @pl.when(sp == 0)
        def _():
            ext[:, :HALO, :] = jnp.zeros((chans // LANES, HALO, LANES), jnp.float32)

    def convolve(layer, half, start, stop):
        base = spans[layer][half][0]
        blocks = []
        while start < stop:
            count = min(ROWS, stop - start)
            blocks.append((start, count))
            start += count

        @pl.loop(0, chans // LANES)
        def _(lane):
            here = pl.ds(pl.multiple_of(lane * LANES, LANES), LANES)
            bias = bias_ref[layer : layer + 1, here]
            for first_row, count in blocks:
                rows = slice(first_row, first_row + count)
                total = jnp.broadcast_to(bias, (count, LANES))
                for tap in range(K):
                    begin = first_row + HALO - K + 1 + tap
                    window = ext[lane, begin : begin + count, :]
                    total = total + window * taps[layer, tap : tap + 1, here]
                filt[rows, here] = total
                inner = slice(first_row - base, first_row - base + count)
                part[half, 0, inner, :] += total
                part[half, 1, inner, :] += total * total

    def stat_copy(layer, half, step, owner, target):
        ref = stat.at[layer, half, owner]
        index = layer * 2 + half
        return remote(ref, ref, stat_send.at[index, step], stat_recv.at[index, step], target)

    def send_stats(layer, half):
        first_row = jnp.sum(jnp.transpose(part[half, 0]), axis=0, keepdims=True)
        square_row = jnp.sum(jnp.transpose(part[half, 1]), axis=0, keepdims=True)
        row_index = lax.broadcasted_iota(jnp.int32, (8, padded), 0)
        stat[layer, half, me] = jnp.where(row_index == 0, first_row, square_row)
        for step in range(1, n_tp):
            copy = stat_copy(layer, half, step, me, lax.rem(me + step, n_tp))
            copy.start()
            pending.append(copy)

    def activate(layer, half, phase):
        for step in range(1, n_tp):
            origin = lax.rem(me + n_tp - step, n_tp)
            stat_copy(layer, half, step, origin, origin).wait_recv()
        totals = jnp.sum(stat[layer, half], axis=0) / total_chans
        mean_row = totals[0:1]
        rstd_row = lax.rsqrt(totals[1:2] - mean_row * mean_row + epsilon)
        column[0] = jnp.transpose(jnp.broadcast_to(mean_row, (LANES, padded)))
        column[1] = jnp.transpose(jnp.broadcast_to(rstd_row, (LANES, padded)))
        start, stop = spans[layer][half]
        for chunk in range(chans // CHUNK):

            @pl.loop(0, (stop - start) // HALO)
            def _(block):
                inner = pl.ds(pl.multiple_of(block * HALO, HALO), HALO)
                rows = pl.ds(pl.multiple_of(start + block * HALO, HALO), HALO)
                for lane in range(CHUNK // LANES):
                    here = slice(chunk * CHUNK + lane * LANES, chunk * CHUNK + (lane + 1) * LANES)
                    values = (filt[rows, here] - column[0, inner, :]) * column[1, inner, :]
                    values = (
                        values * chan_gain_ref[layer : layer + 1, here]
                        + chan_bias_ref[layer : layer + 1, here]
                    )
                    ag[layer, me, chunk, rows, lane * LANES : (lane + 1) * LANES] = (
                        jax.nn.silu(values).astype(jnp.bfloat16)
                    )

            send_own(phase, ag.at[layer], chunk, (start, stop))

    def use_activated(layer):
        def use(owner, chunks, span, first):
            rows = slice(*span)
            total = res[rows, :] if first else acco[rows, :]
            for chunk in chunks:
                start = pl.multiple_of(owner * chans + chunk * CHUNK, LANES)
                total = total + dot_nt(
                    ag[layer, owner, chunk, rows, :], wo[layer, :, pl.ds(start, CHUNK)]
                )
            acco[rows, :] = total

        return use

    def use_stream(owner, chunks, span, first):
        start = pl.multiple_of(owner * feats + chunks[0] * CHUNK, LANES)
        for chunk in chunks:
            prepare(
                1,
                lambda rows, here: sg[owner, chunk, rows, here],
                pl.multiple_of(owner * feats + chunk * CHUNK, LANES),
                CHUNK,
                span,
                (chunk - chunks[0]) * CHUNK,
                first and chunk == 0,
            )
        project(1, start, len(chunks) * CHUNK, span, first)

    n_a, n_f = chans // CHUNK, feats // CHUNK
    part[...] = jnp.zeros(part.shape, jnp.float32)
    for index in range(WEIGHT_PIECES):
        start = index * piece
        prepare(
            0,
            lambda rows, here: x_ref[rows, start + here.start : start + here.stop],
            start,
            piece,
            (0, tokens),
            0,
            index == 0,
        )
        for copy in proj_copies(0, index):
            copy.wait()
        project(0, start, piece, (0, tokens), index == 0)
    res[...] = x_ref[:, pl.ds(pl.multiple_of(me * feats, LANES), feats)].astype(jnp.float32)
    pl.semaphore_wait(
        barrier,
        n_tp - 1 + jnp.where(sp > 0, 1, 0) + jnp.where(sp < n_sp - 1, 1, 0),
    )
    late, early = spans[0]
    send_halo(0)
    gate_rows(0, tokens - HALO)
    convolve(0, 0, *late)
    send_stats(0, 0)
    convolve(0, 1, ROWS, early[1])
    receive_halo(0)
    convolve(0, 1, 0, ROWS)
    send_stats(0, 1)
    activate(0, 0, 0)
    activate(0, 1, 1)
    out_copy(0).wait()
    for half, span in enumerate(spans[0]):
        near(half, ag.at[0], n_a, span, use_activated(0))
        far(half, ag.at[0], n_a, span, use_activated(0))
        rows = slice(*span)
        for chunk in range(n_f):
            here = slice(chunk * CHUNK, (chunk + 1) * CHUNK)
            rounded = acco[rows, here].astype(jnp.bfloat16)
            sg[me, chunk, rows, :] = rounded
            send_own(2 + half, sg, chunk, span)
            res[rows, here] = rounded.astype(jnp.float32)
    part[...] = jnp.zeros(part.shape, jnp.float32)
    for index in range(WEIGHT_PIECES):
        for copy in proj_copies(1, index):
            copy.wait()
    near(2, sg, n_f, late, use_stream)
    far(2, sg, n_f, late, use_stream)
    send_halo(1)
    gate_rows(split, tokens - HALO)
    convolve(1, 0, *spans[1][0])
    send_stats(1, 0)
    near(3, sg, n_f, early, use_stream)
    activate(1, 0, 4)
    far(3, sg, n_f, early, use_stream)
    gate_rows(0, split)
    convolve(1, 1, HALO, spans[1][1][1])
    receive_halo(1)
    convolve(1, 1, 0, HALO)
    send_stats(1, 1)
    out_copy(1).wait()
    near(4, ag.at[1], n_a, spans[1][0], use_activated(1))
    activate(1, 1, 5)
    far(4, ag.at[1], n_a, spans[1][0], use_activated(1))
    near(5, ag.at[1], n_a, spans[1][1], use_activated(1))
    far(5, ag.at[1], n_a, spans[1][1], use_activated(1))
    out_ref[...] = acco[...].astype(jnp.bfloat16)

    @pl.when(sp < n_sp - 1)
    def _():
        for layer in range(LAYERS):
            halo_copy(layer).wait_send()

    for copy in pending:
        copy.wait_send()


def fused(mesh, stream, norm_gain, value_weight, gate_weight, conv_kernel, conv_bias,
          channel_gain, channel_bias, out_weight):
    n_tp, n_sp = mesh.shape["tp"], mesh.shape["sp"]
    width, tokens = stream.shape
    chans, feats = value_weight.shape[1], out_weight.shape[1]
    fits = (
        n_tp % CORES == 0
        and chans % CHUNK == 0
        and feats % CHUNK == 0
        and width % (WEIGHT_PIECES * CHUNK) == 0
        and tokens % ROWS == 0
        and (tokens // 2 - HALO) // HALO * HALO % ROWS == 0
        and tokens >= 4 * ROWS
        and LAYERS == 2
        and n_tp <= 8
    )
    if not fits:
        return local(stream, norm_gain, value_weight, gate_weight, conv_kernel, conv_bias,
                     channel_gain, channel_bias, out_weight)
    split = (tokens // 2 - HALO) // HALO * HALO
    padded = -(-(tokens - split) // LANES) * LANES
    n_y = n_tp // CORES
    n_a, n_f = chans // CHUNK, feats // CHUNK
    most = max(n_a, n_f)
    f32, bf16 = jnp.float32, jnp.bfloat16
    vmem = pl.BlockSpec(memory_space=pltpu.VMEM)
    anyspace = pl.BlockSpec(memory_space=pl.ANY)
    out = pl.pallas_call(
        functools.partial(kernel, n_tp, n_sp),
        out_shape=jax.ShapeDtypeStruct((tokens, feats), bf16),
        in_specs=[vmem] * 6 + [anyspace, anyspace, anyspace],
        out_specs=vmem,
        scratch_shapes=[
            pltpu.VMEM((LAYERS, 2, chans, width), bf16),
            pltpu.VMEM((LAYERS, feats, chans * n_tp), bf16),
            pltpu.VMEM((tokens, max(width // WEIGHT_PIECES, feats)), bf16),
            pltpu.VMEM((chans // LANES, HALO + tokens, LANES), f32),
            pltpu.VMEM((tokens, chans), f32),
            pltpu.VMEM((LAYERS, K, chans), f32),
            pltpu.VMEM((tokens, LANES), f32),
            pltpu.VMEM((2, 2, padded, LANES), f32),
            pltpu.VMEM((2, padded, LANES), f32),
            pltpu.VMEM((LAYERS, HALO, chans), bf16),
            pltpu.VMEM((LAYERS, HALO, chans), bf16),
            pltpu.VMEM((LAYERS, 2, n_tp, 8, padded), f32),
            pltpu.VMEM((LAYERS, n_tp, n_a, tokens, CHUNK), bf16),
            pltpu.VMEM((n_tp, n_f, tokens, CHUNK), bf16),
            pltpu.VMEM((tokens, 2 * chans), f32),
            pltpu.VMEM((tokens, feats), f32),
            pltpu.VMEM((tokens, feats), f32),
            pltpu.SemaphoreType.DMA((LAYERS, WEIGHT_PIECES)),
            pltpu.SemaphoreType.DMA((LAYERS,)),
            pltpu.SemaphoreType.DMA((LAYERS,)),
            pltpu.SemaphoreType.DMA((LAYERS,)),
            pltpu.SemaphoreType.DMA((LAYERS * 2, n_tp)),
            pltpu.SemaphoreType.DMA((LAYERS * 2, n_tp)),
            pltpu.SemaphoreType.DMA((6, n_y, most)),
            pltpu.SemaphoreType.DMA((6, n_y, most)),
            pltpu.SemaphoreType.DMA((6, n_y, most)),
            pltpu.SemaphoreType.DMA((6, n_y, most)),
        ],
        compiler_params=pltpu.CompilerParams(
            collective_id=0, has_side_effects=True, vmem_limit_bytes=60 * 1024 * 1024
        ),
    )(stream.T, norm_gain, conv_kernel, conv_bias, channel_gain, channel_bias,
       value_weight, gate_weight, out_weight)
    return out.T


def solution(mesh):
    placed = (
        P(None, ("grp", "sp")),
        P(),
        P(None, "tp", None),
        P(None, "tp", None),
        P(None, "tp", None),
        P(None, "tp"),
        P(None, "tp"),
        P(None, "tp"),
        P(None, "tp", None),
    )
    return jax.shard_map(
        functools.partial(fused, mesh), mesh=mesh, in_specs=placed, out_specs=P("tp", ("grp", "sp")), check_vma=False
    )
```

time: 66.5 us -> 62.6 us (0.941)
  Pallas kernels: 60.5 us -> 58.2 us
  local copies, waits for them, and re-layouts: 4.96 us -> 3.88 us
  other arithmetic: 0.69 us -> 0 us
    pallas_call x1, Pallas kernels: 60.5 us -> 58.2 us  [fused(): pl.pallas_call(functools.partial(kernel, n_tp, n_sp), out_shape=jax.Shape...]
    broadcast_in_dim x3 -> x0, local copies, waits for them, and re-layouts: 2.07 us -> none  [the longest x1 0.69 us: fused(): conv_bias[:, None]]
    unnamed x2, local copies, waits for them, and re-layouts: 2.89 us -> 3.88 us
    concatenate x1 -> x0, other arithmetic: 0.69 us -> none  [fused(): jnp.concatenate((jnp.swapaxes(conv_kernel, 1, 2), conv_bias[:, None], cha...]
where the time goes in v2:
time: 62.6 us; the launch traced here: 62.1 us
  Pallas kernels  58.2 us (93%)
  local copies, waits for them, and re-layouts  3.88 us (6%)
    pallas_call x1, Pallas kernels, fused(): pl.pallas_call(functools.partial(kernel, n_tp, n_sp), out_shape=jax.Shape...  58.2 us
    unnamed x2, local copies, waits for them, and re-layouts  3.88 us

profile of v2, /device:TPU:1, one launch (start us, length us, event | category | flops | bytes accessed | tf_op | source)
XLA Modules:
  0.0 62.1 jit_solution(17743492324833733323)
XLA Ops:
  0.0 1.9 %copy.10.taps_ref = f32[2,512,31]{2,1,0:T(8,128)} copy(f32[2,512,31]{1,0,2:T(2,128)} %param.13) | data formatting | bytes 253952 | tf_op args[4]
  1.9 58.2 %shard_map.91 = bf16[320,1024]{1,0:T(8,128)(2,1)} custom-call(bf16[320,4096]{1,0:T(8,128)(2,1)} %bitcast.2, f32[2,4096]{1,0:T(2,128)} %gain_ref.1, f32[2,512,31]{2,1,0:T(8,128)} %copy.10.taps_ref, f32[2,512]{1,0:T(2,128)} %bias_ref.1, f32[2,512]{1,0:T(2,128)} %chan_gain_ref.1, f32[2,512]{1,0:T(2,128)} %chan_bias_ref.1, bf16[2,512,4096]{2,1,0:T(8,128)(2,1)} %wv_ref.1, ...), custom_call_target="tpu_custom_call" | custom-call | tf_op jit(solution)/shard_map/pallas_call | solution.py:547
  60.2 2.0 %copy.12 = bf16[1024,320]{0,1:T(8,128)(2,1)} copy(bf16[1024,320]{0,1:T(8,128)(2,1)} %bitcast.3) | data formatting | bytes 1310720

commit v3 on v2

--- a/solution.py
+++ b/solution.py
@@ -208,7 +208,7 @@
         out_copy(layer).start()
 
     for layer in range(LAYERS):
-        taps[layer] = jnp.transpose(taps_ref[layer])
+        taps[layer] = taps_ref[:, layer, :]
 
     def prepare(layer, read, first_col, cols, span, at, first):
         gains = gain_ref[layer : layer + 1, pl.ds(first_col, cols)]
@@ -281,18 +281,28 @@
             f_copy(phase, buf, 0, chunk, sibling, rows).wait_recv()
         use(sibling, range(chunks), span, False)
 
-    def far(phase, buf, chunks, span, use):
+    def arrive(phase, buf, chunk, span, use):
         rows = pl.ds(span[0], span[1] - span[0])
         for step in range(1, n_y):
-            origin = lax.rem(my_y + n_y - step, n_y) * CORES
-            for chunk in range(chunks):
-                y_copy(phase, buf, step, chunk, origin + core, rows).wait_recv()
-                copy = f_copy(phase, buf, step, chunk, origin + core, rows)
-                copy.start()
-                pending.append(copy)
-                use(origin + core, (chunk,), span, False)
-                f_copy(phase, buf, step, chunk, origin + 1 - core, rows).wait_recv()
-                use(origin + 1 - core, (chunk,), span, False)
+            owner = lax.rem(my_y + n_y - step, n_y) * CORES + core
+            y_copy(phase, buf, step, chunk, owner, rows).wait_recv()
+            copy = f_copy(phase, buf, step, chunk, owner, rows)
+            copy.start()
+            pending.append(copy)
+            use(owner, (chunk,), span, False)
+
+    def relayed(phase, buf, chunk, span, use):
+        rows = pl.ds(span[0], span[1] - span[0])
+        for step in range(1, n_y):
+            owner = lax.rem(my_y + n_y - step, n_y) * CORES + 1 - core
+            f_copy(phase, buf, step, chunk, owner, rows).wait_recv()
+            use(owner, (chunk,), span, False)
+
+    def far(phase, buf, chunks, span, use):
+        for chunk in chunks:
+            arrive(phase, buf, chunk, span, use)
+            if chunk > 0:
+                relayed(phase, buf, chunk - 1, span, use)
 
     def gate(first_row, count):
         rows = pl.ds(first_row, count)
@@ -472,9 +482,7 @@
     activate(0, 0, 0)
     activate(0, 1, 1)
     out_copy(0).wait()
-    for half, span in enumerate(spans[0]):
-        near(half, ag.at[0], n_a, span, use_activated(0))
-        far(half, ag.at[0], n_a, span, use_activated(0))
+    def send_stream(half, span):
         rows = slice(*span)
         for chunk in range(n_f):
             here = slice(chunk * CHUNK, (chunk + 1) * CHUNK)
@@ -482,30 +490,46 @@
             sg[me, chunk, rows, :] = rounded
             send_own(2 + half, sg, chunk, span)
             res[rows, here] = rounded.astype(jnp.float32)
+
+    use = use_activated(0)
+    near(0, ag.at[0], n_a, late, use)
+    far(0, ag.at[0], range(n_a), late, use)
+    near(1, ag.at[0], n_a, early, use)
+    relayed(0, ag.at[0], n_a - 1, late, use)
+    send_stream(0, late)
+    far(1, ag.at[0], range(n_a), early, use)
     part[...] = jnp.zeros(part.shape, jnp.float32)
     for index in range(WEIGHT_PIECES):
         for copy in proj_copies(1, index):
             copy.wait()
     near(2, sg, n_f, late, use_stream)
-    far(2, sg, n_f, late, use_stream)
+    relayed(1, ag.at[0], n_a - 1, early, use)
+    send_stream(1, early)
+    far(2, sg, range(n_f), late, use_stream)
+    near(3, sg, n_f, early, use_stream)
+    relayed(2, sg, n_f - 1, late, use_stream)
     send_halo(1)
     gate_rows(split, tokens - HALO)
     convolve(1, 0, *spans[1][0])
     send_stats(1, 0)
-    near(3, sg, n_f, early, use_stream)
+    far(3, sg, range(n_f // 2), early, use_stream)
     activate(1, 0, 4)
-    far(3, sg, n_f, early, use_stream)
+    far(3, sg, range(n_f // 2, n_f), early, use_stream)
+    relayed(3, sg, n_f - 1, early, use_stream)
     gate_rows(0, split)
     convolve(1, 1, HALO, spans[1][1][1])
     receive_halo(1)
     convolve(1, 1, 0, HALO)
     send_stats(1, 1)
     out_copy(1).wait()
-    near(4, ag.at[1], n_a, spans[1][0], use_activated(1))
+    use = use_activated(1)
+    near(4, ag.at[1], n_a, spans[1][0], use)
     activate(1, 1, 5)
-    far(4, ag.at[1], n_a, spans[1][0], use_activated(1))
-    near(5, ag.at[1], n_a, spans[1][1], use_activated(1))
-    far(5, ag.at[1], n_a, spans[1][1], use_activated(1))
+    far(4, ag.at[1], range(n_a), spans[1][0], use)
+    near(5, ag.at[1], n_a, spans[1][1], use)
+    relayed(4, ag.at[1], n_a - 1, spans[1][0], use)
+    far(5, ag.at[1], range(n_a), spans[1][1], use)
+    relayed(5, ag.at[1], n_a - 1, spans[1][1], use)
     out_ref[...] = acco[...].astype(jnp.bfloat16)
 
     @pl.when(sp < n_sp - 1)
@@ -581,7 +605,7 @@
         compiler_params=pltpu.CompilerParams(
             collective_id=0, has_side_effects=True, vmem_limit_bytes=60 * 1024 * 1024
         ),
-    )(stream.T, norm_gain, conv_kernel, conv_bias, channel_gain, channel_bias,
+    )(stream.T, norm_gain, jnp.transpose(conv_kernel, (2, 0, 1)), conv_bias, channel_gain, channel_bias,
        value_weight, gate_weight, out_weight)
     return out.T
 

time: 62.6 us -> 57.5 us (0.919)
  Pallas kernels: 58.2 us -> 55.3 us
  local copies, waits for them, and re-layouts: 3.88 us -> 1.97 us
    pallas_call x1, Pallas kernels: 58.2 us -> 55.3 us  [fused(): pl.pallas_call(functools.partial(kernel, n_tp, n_sp), out_shape=jax.Shape...]
    unnamed x2 -> x1, local copies, waits for them, and re-layouts: 3.88 us -> 1.97 us
where the time goes in v3:
time: 57.5 us; the launch traced here: 57.3 us
  Pallas kernels  55.3 us (96%)
  local copies, waits for them, and re-layouts  1.97 us (3%)
    pallas_call x1, Pallas kernels, fused(): pl.pallas_call(functools.partial(kernel, n_tp, n_sp), out_shape=jax.Shape...  55.3 us
    unnamed x1, local copies, waits for them, and re-layouts  1.97 us

profile of v3, /device:TPU:1, one launch (start us, length us, event | category | flops | bytes accessed | tf_op | source)
XLA Modules:
  0.0 57.3 jit_solution(17792574597654737181)
XLA Ops:
  0.0 55.3 %shard_map.91 = bf16[320,1024]{1,0:T(8,128)(2,1)} custom-call(bf16[320,4096]{1,0:T(8,128)(2,1)} %bitcast.3, f32[2,4096]{1,0:T(2,128)} %gain_ref.1, f32[31,2,512]{2,1,0:T(2,128)} %bitcast.5, f32[2,512]{1,0:T(2,128)} %bias_ref.1, f32[2,512]{1,0:T(2,128)} %chan_gain_ref.1, f32[2,512]{1,0:T(2,128)} %chan_bias_ref.1, bf16[2,512,4096]{2,1,0:T(8,128)(2,1)} %wv_ref.1, ...), custom_call_target="tpu_custom_call" | custom-call | tf_op jit(solution)/shard_map/pallas_call | solution.py:571
  55.3 2.0 %copy.11 = bf16[1024,320]{0,1:T(8,128)(2,1)} copy(bf16[1024,320]{0,1:T(8,128)(2,1)} %bitcast.4) | data formatting | bytes 1310720

commit v4 on v3

--- a/solution.py
+++ b/solution.py
@@ -539,6 +539,10 @@
 
     for copy in pending:
         copy.wait_send()
+
+
+def hand_over(from_ref, to_ref):
+    to_ref[...] = from_ref[...]
 
 
 def fused(mesh, stream, norm_gain, value_weight, gate_weight, conv_kernel, conv_bias,
@@ -607,6 +611,12 @@
         ),
     )(stream.T, norm_gain, jnp.transpose(conv_kernel, (2, 0, 1)), conv_bias, channel_gain, channel_bias,
        value_weight, gate_weight, out_weight)
+    out = pl.pallas_call(
+        hand_over,
+        out_shape=jax.ShapeDtypeStruct(out.shape, out.dtype),
+        in_specs=[vmem],
+        out_specs=vmem,
+    )(out)
     return out.T
 
 

time: 57.5 us -> 57.5 us (level)
  Pallas kernels: 55.3 us -> 57.3 us
  local copies, waits for them, and re-layouts: 1.97 us -> 0 us
    pallas_call x0 -> x1, Pallas kernels: none -> 1.97 us  [fused(): pl.pallas_call(hand_over, out_shape=jax.ShapeDtypeStruct(out.shape, out.d...]
    unnamed x1 -> x0, local copies, waits for them, and re-layouts: 1.97 us -> none
where the time goes in v4:
time: 57.5 us; the launch traced here: 57.3 us
  Pallas kernels  57.3 us (100%)
    pallas_call x1, Pallas kernels, fused(): pl.pallas_call(functools.partial(kernel, n_tp, n_sp), out_shape=jax.Shape...  55.3 us
    pallas_call x1, Pallas kernels, fused(): pl.pallas_call(hand_over, out_shape=jax.ShapeDtypeStruct(out.shape, out.d...  1.97 us

profile of v4, /device:TPU:1, one launch (start us, length us, event | category | flops | bytes accessed | tf_op | source)
XLA Modules:
  0.0 57.3 jit_solution(560951425407099456)
XLA Ops:
  0.0 55.3 %shard_map.91.from_ref = bf16[320,1024]{1,0:T(8,128)(2,1)} custom-call(bf16[320,4096]{1,0:T(8,128)(2,1)} %bitcast.3, f32[2,4096]{1,0:T(2,128)} %gain_ref.1, f32[31,2,512]{2,1,0:T(2,128)} %bitcast.4, f32[2,512]{1,0:T(2,128)} %bias_ref.1, f32[2,512]{1,0:T(2,128)} %chan_gain_ref.1, f32[2,512]{1,0:T(2,128)} %chan_bias_ref.1, bf16[2,512,4096]{2,1,0:T(8,128)(2,1)} %wv_ref.1, ...), custom_call_target="tpu_custom_call" | custom-call | tf_op jit(solution)/shard_map/pallas_call | solution.py:575
  55.3 2.0 %shard_map.92 = bf16[320,1024]{1,0:T(8,128)(2,1)} custom-call(bf16[320,1024]{1,0:T(8,128)(2,1)} %shard_map.91.from_ref), custom_call_target="tpu_custom_call" | custom-call | tf_op jit(solution)/shard_map/pallas_call | solution.py:614
